TPU v7x, 32 devices: a whole 2x2x4 slice. The times are simulated.
32 devices in a mesh: sp: 16 (over z, y, x), tp: 2 (over core).
Axes of the slice: x: 2, y: 2, z: 4, core: 2. Of those that a mesh axis runs over, the one named last changes fastest.
Arguments:
- resid: bfloat16 [6144, 2048], P('sp'), may hold values from -6 to 6
- x_branch: bfloat16 [6144, 2048], P('sp', 'tp'), may hold values from -6 to 6
- gate_branch: bfloat16 [6144, 2048], P('sp', 'tp'), may hold values from -6 to 6
- conv_w: float32 [4, 2048], P(None, 'tp'), may hold values from -3 to 3
- gate_a_w: bfloat16 [32, 64, 64], P('tp'), may hold values from -0.75 to 0.75
- gate_x_w: bfloat16 [32, 64, 64], P('tp'), may hold values from -0.75 to 0.75
- decay_rate: float32 [2048], P('tp'), may hold values from 0 to 0.01, as said below
- decay_extra: float32 [6144, 2048], P('sp', 'tp'), may hold values from -3 to 0, as said below
- w_proj: bfloat16 [2048, 2048], P('tp'), may hold values from -0.125 to 0.125
- mix_gain: float32 [2048], replicated, may hold values from 0.1 to 1.9
- pre_gain: float32 [2048], replicated, may hold values from 0.1 to 1.9
- w_gate: bfloat16 [2048, 5632], P('sp', 'tp'), may hold values from -0.125 to 0.125
- w_up: bfloat16 [2048, 5632], P('sp', 'tp'), may hold values from -0.125 to 0.125
- w_down: bfloat16 [5632, 2048], P('tp', 'sp'), may hold values from -0.078125 to 0.078125
- out_gain: float32 [2048], replicated, may hold values from 0.1 to 1.9
Outputs:
- stream_out: bfloat16 [6144, 2048], P(('sp', 'tp'))
Inputs may be any that keep to these rules, and one draw needn't show every extreme that they name: `decay_rate`: positive rates. `decay_extra`: non-positive values.
All inputs are finite; a program needn't handle non-finite values.
Results may differ from a plain program's by a relative error of at most 0.015.
Values may be sent and summed in bfloat16 or wider, within the bound.
A program may use at most 128 MiB of HBM per device.

v0:
```python
import jax
import jax.numpy as jnp
from jax import lax
from jax.sharding import PartitionSpec as P

LRU_SCALE = 8.0
NORM_EPS = 1e-06


def from_behind(value, axis, steps):
    count = lax.axis_size(axis)
    first, last = (max(0, -steps), min(count, count - steps))
    return lax.ppermute(value, axis, [(source, source + steps) for source in range(first, last)])


def prefix(part, axis, combine, identity):
    place = lax.axis_index(axis)
    gathered = jax.tree.map(lambda a: lax.all_gather(a, axis), part)
    state = jax.tree.map(lambda a, e: jnp.zeros_like(a) + jnp.asarray(e, a.dtype), part, identity)

    def one(turn, state):
        return combine(
            state, jax.tree.map(lambda a: lax.dynamic_index_in_dim(a, turn, 0, False), gathered)
        )

    return lax.fori_loop(0, place, one, state)


def chain(earlier, later):
    return (earlier[0] * later[0], later[0] * earlier[1] + later[1])


def rms_scale(values, gains):
    return values * lax.rsqrt(jnp.mean(values * values, axis=-1, keepdims=True) + NORM_EPS) * gains


def shards(
    resid,
    x_branch,
    gate_branch,
    conv_w,
    gate_a_w,
    gate_x_w,
    decay_rate,
    decay_extra,
    w_proj,
    mix_gain,
    pre_gain,
    w_gate,
    w_up,
    w_down,
    out_gain,
):
    length = x_branch.shape[0]
    width = x_branch.shape[1]
    taps = conv_w.shape[0]
    before = from_behind(x_branch[length - (taps - 1) :], "sp", 1)
    padded = jnp.concatenate([before, x_branch], axis=0).astype(jnp.float32)
    conv = padded[0:length] * conv_w[0]
    for tap in range(1, taps):
        conv = conv + padded[tap : tap + length] * conv_w[tap]
    conv_out = conv.astype(jnp.bfloat16)
    nblocks = gate_a_w.shape[0]
    grouped = conv_out.reshape(length, nblocks, gate_a_w.shape[1])
    recur = jax.nn.sigmoid(
        jnp.einsum("rnc,ncd->rnd", grouped, gate_a_w, preferred_element_type=jnp.float32).reshape(
            length, width
        )
    )
    inject = jax.nn.sigmoid(
        jnp.einsum("rnc,ncd->rnd", grouped, gate_x_w, preferred_element_type=jnp.float32).reshape(
            length, width
        )
    )
    log_decay = -LRU_SCALE * recur * decay_rate + decay_extra
    decay = jnp.exp(log_decay)
    drive = jnp.sqrt(-jnp.expm1(2.0 * log_decay)) * inject * conv_out.astype(jnp.float32)
    prod_local, state_local = lax.associative_scan(chain, (decay, drive), axis=0)
    identity = (jnp.ones((width,), jnp.float32), jnp.zeros((width,), jnp.float32))
    carried = prefix((prod_local[-1], state_local[-1]), "sp", chain, identity)
    state = state_local + prod_local * carried[1][None, :]
    mixer = (state * jax.nn.gelu(gate_branch.astype(jnp.float32))).astype(jnp.bfloat16)
    share_rows = length // lax.axis_size("tp")
    first = lax.axis_index("tp") * share_rows
    mixed = lax.psum(
        jnp.dot(mixer, w_proj, preferred_element_type=jnp.float32).astype(jnp.bfloat16), "tp"
    ).astype(jnp.float32)
    stream = resid.astype(jnp.float32) + rms_scale(mixed, mix_gain)
    normed = rms_scale(stream, pre_gain).astype(jnp.bfloat16)
    after_mix = lax.dynamic_slice_in_dim(stream, first, share_rows, 0)
    gate_full, up_full = (
        lax.all_gather(w_gate, "sp", axis=0, tiled=True),
        lax.all_gather(w_up, "sp", axis=0, tiled=True),
    )
    down_full = lax.all_gather(w_down, "sp", axis=1, tiled=True)
    gate = jnp.dot(normed, gate_full, preferred_element_type=jnp.float32)
    upward = jnp.dot(normed, up_full, preferred_element_type=jnp.float32)
    hidden = (jax.nn.silu(gate) * upward).astype(jnp.bfloat16)
    ffn = lax.psum_scatter(
        jnp.dot(hidden, down_full, preferred_element_type=jnp.float32).astype(jnp.bfloat16),
        "tp",
        scatter_dimension=0,
        tiled=True,
    ).astype(jnp.float32)
    return (after_mix + 0.5 * rms_scale(ffn, out_gain)).astype(jnp.bfloat16)


def solution(mesh):
    return jax.shard_map(
        shards,
        mesh=mesh,
        in_specs=(
            P("sp", None),
            P("sp", "tp"),
            P("sp", "tp"),
            P(None, "tp"),
            P("tp", None, None),
            P("tp", None, None),
            P("tp"),
            P("sp", "tp"),
            P("tp", None),
            P(),
            P(),
            P("sp", "tp"),
            P("sp", "tp"),
            P("tp", "sp"),
            P(),
        ),
        out_specs=P(("sp", "tp"), None),
        check_vma=False,
    )
```

profile of v0, /device:TPU:0, one launch (start us, length us, event | category | flops | bytes accessed | tf_op | source)
XLA Modules:
  0.0 737.7 jit_solution(13793167642620603508)
XLA Ops:
  8.1 4.9 collective-permute-start
  17.8 1.8 add_divide_fusion.1
  19.6 1.7 copy.106
  21.3 1.8 add_divide_fusion
  23.0 1.6 copy.108
  24.6 5.3 convert_multiply_fusion.7
  30.0 4.5 slice.281
  34.4 2.1 slice.282
  36.6 2.1 slice.280
  38.7 2.2 slice.284
  40.9 3.4 multiply_add_fusion.2
  44.2 2.7 slice.287
  46.9 2.7 slice.288
  49.6 2.7 slice.286
  52.4 2.7 slice.290
  55.1 2.4 multiply_add_fusion.3
  57.4 1.7 slice.293
  59.1 1.7 slice.294
  60.8 1.7 slice.292
  62.5 1.7 slice.296
  64.1 2.0 multiply_add_fusion.4
  67.4 1.6 slice.298
  69.0 1.6 slice.302
  70.6 1.7 multiply_add_fusion.5
  76.6 1.6 multiply_add_fusion.6
  102.2 1.7 slice.291
  103.9 1.7 slice.334
  108.2 2.7 slice.285
  111.0 2.8 slice.336
  116.5 2.3 slice.279
  118.8 2.2 slice.338
  128.0 3.1 pad.113
  135.6 3.2 pad.112
  139.6 42.0 %all-gather.1 = f32[16,1,1024]{2,1,0:T(1,128)S(1)} all-gather(f32[1,1,1024]{2,1,0:T(1,128)S(1)} %add_bitcast_fusion), channel_id=1, replica_groups=mesh['sp'=16,'tp'=2] {'sp'}, dimensions={0}, use_global_device_ids=true | all-gather | bytes 69632 | tf_op jit(solution)/shard_map/all_gather | solution.py:18
  181.7 3.1 pad.129
  184.9 3.2 pad.128
  188.9 35.8 %all-gather = f32[16,1,1024]{2,1,0:T(1,128)S(1)} all-gather(f32[1,1,1024]{2,1,0:T(1,128)S(1)} %add_bitcast_fusion.1), channel_id=1, replica_groups=mesh['sp'=16,'tp'=2] {'sp'}, dimensions={0}, use_global_device_ids=true | all-gather | bytes 69632 | tf_op jit(solution)/shard_map/all_gather | solution.py:18
  224.7 7.0 convolution_convert_fusion.1
  233.6 17.4 %all-reduce.34.cloned.1.call-done = bf16[384,2048]{1,0:T(8,128)(2,1)} async-done(((bf16[384,2048]{1,0:T(8,128)(2,1)}), bf16[384,2048]{1,0:T(8,128)(2,1)}) %all-reduce.34.cloned.1.call-update) | async-done | bytes 1572880 | tf_op jit(solution)/shard_map/psum | solution.py:85
  250.9 1.9 fusion.1
  252.9 2.3 multiply_reduce_fusion
  255.2 119.6 %all-gather.6.cloned.1.call-done = bf16[2048,2816]{1,0:T(8,128)(2,1)} async-done(((bf16[128,2816]{1,0:T(8,128)(2,1)}), bf16[2048,2816]{1,0:T(8,128)(2,1)}) %all-gather.6.cloned.1.call-update) | async-done | bytes 11534352 | tf_op jit(solution)/shard_map/all_gather | solution.py:92
  374.9 9.6 %fusion.43 = f32[384,2816]{1,0:T(8,128)} fusion(bf16[2048,2816]{1,0:T(8,128)(2,1)} %all-gather.6.cloned.1.call-done, f32[384,2048]{1,0:T(8,128)S(1)} %get-tuple-element.61, f32[2048]{0:T(1024)S(1)} %copy-done.38, f32[384]{0:T(512)S(1)} %add_rsqrt_fusion), kind=kOutput, calls=%fused_computation.118 | convolution fusion | flops 4431544320 | bytes 19015168 | tf_op jit(solution)/shard_map/dot_general | solution.py:96
  384.4 173.1 %all-gather.10.cloned.1.call-done = bf16[2816,2048]{1,0:T(8,128)(2,1)} async-done(((bf16[2816,128]{1,0:T(8,128)(2,1)}), bf16[2816,2048]{1,0:T(8,128)(2,1)}) %all-gather.10.cloned.1.call-update) | async-done | bytes 11534352 | tf_op jit(solution)/shard_map/all_gather | solution.py:95
  557.5 142.0 %all-gather.8.cloned.1.call-done = bf16[2048,2816]{1,0:T(8,128)(2,1)} async-done(((bf16[128,2816]{1,0:T(8,128)(2,1)}), bf16[2048,2816]{1,0:T(8,128)(2,1)}) %all-gather.8.cloned.1.call-update) | async-done | bytes 11534352 | tf_op jit(solution)/shard_map/all_gather | solution.py:93
  699.5 19.3 %convolution_convert_fusion = bf16[384,2048]{1,0:T(8,128)(2,1)} fusion(bf16[2816,2048]{1,0:T(8,128)(2,1)} %all-gather.10.cloned.1.call-done, bf16[2048,2816]{1,0:T(8,128)(2,1)} %all-gather.8.cloned.1.call-done, f32[384,2816]{1,0:T(8,128)} %fusion.43, f32[384,2048]{1,0:T(8,128)S(1)} %get-tuple-element.61, f32[2048]{0:T(1024)S(1)} %copy-done.38, ...), kind=kOutput, calls=%fused_computation.12 | convolution fusion | flops 8868003840 | bytes 32122368 | tf_op jit(solution)/shard_map/dot_general | solution.py:100
  718.9 7.4 reduce-scatter.2.cloned.1.call-done
  727.7 2.4 fusion.8
  (205 shorter events, 56.4 us)
Async XLA Ops:
  7.4 10.4 %copy-start = (bf16[16,64,64]{2,1,0:T(8,128)(2,1)S(1)}, bf16[16,64,64]{2,1,0:T(8,128)(2,1)}, u32[]{:S(2)}) copy-start(bf16[16,64,64]{2,1,0:T(8,128)(2,1)} %param.21) | copy-start | bytes 393220
  7.4 243.6 %all-reduce.34.cloned.1.call-start = ((), (), s32[]{:S(2)}) async-start(), calls=%async_computation.1 | async-start | bytes 3145728 | tf_op jit(solution)/shard_map/psum | solution.py:85
  8.1 6.5 collective-permute-start
  19.6 1.7 copy-start.37
  29.9 4.5 copy-start.2
  116.5 5.7 copy-start.15
  116.5 5.7 copy-start.16
  116.5 5.7 copy-start.17
  116.5 6.0 copy-start.18
  116.5 6.0 copy-start.19
  116.5 6.0 copy-start.26
  116.5 6.0 copy-start.27
  118.8 3.8 copy-start.14
  118.8 3.9 copy-start.33
  118.8 3.9 copy-start.32
  121.6 2.1 copy-start.31
  122.2 1.6 copy-start.30
  122.6 1.3 copy-start.13
  122.8 1.2 copy-start.29
  123.7 0.7 copy-start.28
  124.0 0.9 copy-start.11
  124.0 1.0 copy-start.12
  124.5 0.7 copy-start.25
  125.0 0.7 copy-start.24
  125.7 1.0 copy-start.9
  125.7 1.2 copy-start.10
  126.9 0.7 copy-start.23
  128.0 3.1 copy-start.22
  132.5 1.4 copy-start.4
  132.5 1.6 copy-start.5
  134.1 1.4 copy-start.21
  135.6 3.2 copy-start.8
  135.6 46.1 %copy-start.7 = (f32[192,1024]{1,0:T(8,128)S(1)}, f32[192,1024]{1,0:T(8,128)}, u32[]{:S(2)}) copy-start(f32[192,1024]{1,0:T(8,128)} %add.291) | copy-start | bytes 2359300
  138.8 46.0 %copy-start.6 = (f32[191,1024]{1,0:T(8,128)S(1)}, f32[191,1024]{1,0:T(8,128)}, u32[]{:S(2)}) copy-start(f32[191,1024]{1,0:T(8,128)} %get-tuple-element.71) | copy-start | bytes 2347012
  138.8 46.0 %copy-start.20 = (f32[1,1024]{1,0:T(1,128)S(1)}, f32[1,1024]{1,0:T(1,128)}, u32[]{:S(2)}) copy-start(f32[1,1024]{1,0:T(1,128)} %slice.386) | copy-start | bytes 12292
  184.9 39.8 %copy-start.36 = (bf16[384,1024]{1,0:T(8,128)(2,1)S(1)}, bf16[384,1024]{1,0:T(8,128)(2,1)}, u32[]{:S(2)}) copy-start(bf16[384,1024]{1,0:T(8,128)(2,1)} %param.19) | copy-start | bytes 2359300
  231.8 143.1 %all-gather.6.cloned.1.call-start = ((), (), s32[]{:S(2)}) async-start(), calls=%async_computation.2 | async-start | bytes 12255232 | tf_op jit(solution)/shard_map/all_gather | solution.py:92
  232.3 20.5 %copy-start.34 = (f32[2048]{0:T(1024)S(1)}, f32[2048]{0:T(1024)}, u32[]{:S(2)}) copy-start(f32[2048]{0:T(1024)} %param.26) | copy-start | bytes 24580
  232.3 325.2 %all-gather.10.cloned.1.call-start = ((), (), s32[]{:S(2)}) async-start(), calls=%async_computation.4 | async-start | bytes 12255232 | tf_op jit(solution)/shard_map/all_gather | solution.py:95
  232.9 466.6 %all-gather.8.cloned.1.call-start = ((), (), s32[]{:S(2)}) async-start(), calls=%async_computation.3 | async-start | bytes 12255232 | tf_op jit(solution)/shard_map/all_gather | solution.py:93
  233.5 492.8 %reduce-scatter.2.cloned.1.call-start = ((), (), s32[]{:S(2)}) async-start(), calls=%async_computation.5 | async-start | bytes 2359296 | tf_op jit(solution)/shard_map/reduce_scatter | solution.py:99
  250.9 1.9 copy-start.3
  252.9 122.0 %copy-start.38 = (f32[2048]{0:T(1024)S(1)}, f32[2048]{0:T(1024)}, u32[]{:S(2)}) copy-start(f32[2048]{0:T(1024)} %param.27) | copy-start | bytes 24580
  718.9 8.8 %copy-start.35 = (f32[2048]{0:T(1024)S(1)}, f32[2048]{0:T(1024)}, u32[]{:S(2)}) copy-start(f32[2048]{0:T(1024)} %param.31) | copy-start | bytes 24580
  727.7 2.4 copy-start.1
Sparse Core Ops, SparseCore 0:
  231.9 19.0 all-reduce.33
  719.0 7.2 reduce-scatter.1
Sparse Core Ops, SparseCore 1:
  235.0 139.8 all-gather.5
  377.4 180.0 all-gather.9
  560.1 139.3 all-gather.7
where the time goes:
time: 740 us; the launch traced here: 738 us
  waiting for transfers between devices  461 us (62%)
  local copies, waits for them, and re-layouts  103 us (14%)
  blocking collectives  77.8 us (11%)
  matrix products  39.4 us (5%)
  other arithmetic  35.2 us (5%)
  between operations  15.9 us (2%)
    all_gather x1, waiting for transfers between devices, shards(): down_full = lax.all_gather(w_down, 'sp', axis=1, tiled=True)  173 us
    all_gather x1, waiting for transfers between devices, shards(): lax.all_gather(w_up, 'sp', axis=0, tiled=True)  142 us
    all_gather x1, waiting for transfers between devices, shards(): lax.all_gather(w_gate, 'sp', axis=0, tiled=True)  120 us
    slice x56, local copies, waits for them, and re-layouts, shards(): lax.associative_scan(chain, (decay, drive), axis=0)  79.8 us
    all_gather x2, blocking collectives, prefix(): gathered = jax.tree.map(lambda a: lax.all_gather(a, axis), part)  77.8 us
    dot_general x1, matrix products, shards(): jnp.dot(hidden, down_full, preferred_element_type=jnp.float32)  19.3 us
    psum x1, waiting for transfers between devices, shards(): lax.psum(jnp.dot(mixer, w_proj, preferred_element_type=jnp.float32).astyp...  17.4 us
    add x15, other arithmetic, chain(): return (earlier[0] * later[0], later[0] * earlier[1] + later[1])  15 us
  transfers between devices with their start and end apart: 6, of which 5 were waited for; matrix products, arithmetic and copies ran while one was open for 2% of the time, Pallas kernels for 0%

commit v1 on v0

--- a/solution.py
+++ b/solution.py
@@ -92,7 +92,7 @@
         lax.all_gather(w_gate, "sp", axis=0, tiled=True),
         lax.all_gather(w_up, "sp", axis=0, tiled=True),
     )
-    down_full = lax.all_gather(w_down, "sp", axis=1, tiled=True)
+    down_full = jnp.concatenate(lax.all_gather(w_down, "sp"), axis=1)
     gate = jnp.dot(normed, gate_full, preferred_element_type=jnp.float32)
     upward = jnp.dot(normed, up_full, preferred_element_type=jnp.float32)
     hidden = (jax.nn.silu(gate) * upward).astype(jnp.bfloat16)

time: 740 us -> 702 us (0.949)
  waiting for transfers between devices: 461 us -> 405 us
  local copies, waits for them, and re-layouts: 103 us -> 118 us
    all_gather x1, waiting for transfers between devices: 173 us -> 120 us  [shards(): down_full = jnp.concatenate(lax.all_gather(w_down, 'sp'), axis=1)]
    reshape x0 -> x1, local copies, waits for them, and re-layouts: none -> 15.2 us  [shards(): down_full = jnp.concatenate(lax.all_gather(w_down, 'sp'), axis=1)]
    all_gather x1, waiting for transfers between devices: 142 us -> 132 us  [shards(): lax.all_gather(w_up, 'sp', axis=0, tiled=True)]
  transfers between devices with their start and end apart: 6 -> 6, of which waited for: 5 -> 5; matrix products, arithmetic and copies ran while one was open for 2% -> 4% of each run, Pallas kernels for 0% -> 0%
where the time goes in v1:
time: 702 us; the launch traced here: 699 us
  waiting for transfers between devices  405 us (58%)
  local copies, waits for them, and re-layouts  118 us (17%)
  blocking collectives  77.8 us (11%)
  matrix products  41.7 us (6%)
  other arithmetic  35.2 us (5%)
  between operations  15.9 us (2%)
    all_gather x1, waiting for transfers between devices, shards(): lax.all_gather(w_up, 'sp', axis=0, tiled=True)  132 us
    all_gather x1, waiting for transfers between devices, shards(): lax.all_gather(w_gate, 'sp', axis=0, tiled=True)  127 us
    all_gather x1, waiting for transfers between devices, shards(): down_full = jnp.concatenate(lax.all_gather(w_down, 'sp'), axis=1)  120 us
    slice x56, local copies, waits for them, and re-layouts, shards(): lax.associative_scan(chain, (decay, drive), axis=0)  79.8 us
    all_gather x2, blocking collectives, prefix(): gathered = jax.tree.map(lambda a: lax.all_gather(a, axis), part)  77.8 us
    dot_general x1, matrix products, shards(): jnp.dot(hidden, down_full, preferred_element_type=jnp.float32)  21.5 us
    psum x1, waiting for transfers between devices, shards(): lax.psum(jnp.dot(mixer, w_proj, preferred_element_type=jnp.float32).astyp...  17.4 us
    reshape x1, local copies, waits for them, and re-layouts, shards(): down_full = jnp.concatenate(lax.all_gather(w_down, 'sp'), axis=1)  15.2 us
  transfers between devices with their start and end apart: 6, of which 5 were waited for; matrix products, arithmetic and copies ran while one was open for 4% of the time, Pallas kernels for 0%

profile of v1, /device:TPU:0, one launch (start us, length us, event | category | flops | bytes accessed | tf_op | source)
XLA Modules:
  0.0 699.2 jit_solution(6892880732078877363)
XLA Ops:
  8.1 4.9 collective-permute-start
  17.8 1.8 add_divide_fusion.1
  19.6 1.7 copy.110
  21.3 1.8 add_divide_fusion
  23.0 1.6 copy.112
  24.6 5.3 convert_multiply_fusion.7
  30.0 4.5 slice.281
  34.4 2.1 slice.282
  36.6 2.1 slice.280
  38.7 2.2 slice.284
  40.9 3.4 multiply_add_fusion.2
  44.2 2.7 slice.287
  46.9 2.7 slice.288
  49.6 2.7 slice.286
  52.4 2.7 slice.290
  55.1 2.4 multiply_add_fusion.3
  57.4 1.7 slice.293
  59.1 1.7 slice.294
  60.8 1.7 slice.292
  62.5 1.7 slice.296
  64.1 2.0 multiply_add_fusion.4
  67.4 1.6 slice.298
  69.0 1.6 slice.302
  70.6 1.7 multiply_add_fusion.5
  102.2 1.7 slice.291
  103.9 1.7 slice.334
  108.2 2.7 slice.285
  111.0 2.8 slice.336
  116.5 2.3 slice.279
  118.8 2.2 slice.338
  128.0 3.1 pad.113
  135.6 3.2 pad.112
  139.6 42.0 %all-gather.2 = f32[16,1,1024]{2,1,0:T(1,128)S(1)} all-gather(f32[1,1,1024]{2,1,0:T(1,128)S(1)} %add_bitcast_fusion), channel_id=1, replica_groups=mesh['sp'=16,'tp'=2] {'sp'}, dimensions={0}, use_global_device_ids=true | all-gather | bytes 69632 | tf_op jit(solution)/shard_map/all_gather | solution.py:18
  181.7 3.1 pad.129
  184.9 3.2 pad.128
  188.9 35.8 %all-gather.1 = f32[16,1,1024]{2,1,0:T(1,128)S(1)} all-gather(f32[1,1,1024]{2,1,0:T(1,128)S(1)} %add_bitcast_fusion.1), channel_id=1, replica_groups=mesh['sp'=16,'tp'=2] {'sp'}, dimensions={0}, use_global_device_ids=true | all-gather | bytes 69632 | tf_op jit(solution)/shard_map/all_gather | solution.py:18
  224.7 7.0 %convolution_convert_fusion.1 = bf16[384,2048]{1,0:T(8,128)(2,1)} fusion(bf16[1024,2048]{1,0:T(8,128)(2,1)} %param.25, bf16[384,1024]{1,0:T(8,128)(2,1)S(1)} %copy-done.36, f32[384,1024]{1,0:T(8,128)} %pad.128, f32[384,1024]{1,0:T(8,128)} %pad.129, f32[384,1024]{1,0:T(8,128)} %pad.112, f32[384,1024]{1,0:T(8,128)S(1)} %copy-done.8, ...), kind=kOutput, calls=%fused_computation.13 | convolution fusion | flops 1617297408 | bytes 12849152 | tf_op jit(solution)/shard_map/dot_general | solution.py:86
  233.6 17.4 %all-reduce.34.cloned.1.call-done = bf16[384,2048]{1,0:T(8,128)(2,1)} async-done(((bf16[384,2048]{1,0:T(8,128)(2,1)}), bf16[384,2048]{1,0:T(8,128)(2,1)}) %all-reduce.34.cloned.1.call-update) | async-done | bytes 1572880 | tf_op jit(solution)/shard_map/psum | solution.py:85
  250.9 1.9 fusion.1
  252.9 2.3 multiply_reduce_fusion
  255.2 119.6 %all-gather.11.cloned.1.call-done = bf16[45056,128]{1,0:T(8,128)(2,1)} async-done(((bf16[2816,128]{1,0:T(8,128)(2,1)}), bf16[45056,128]{1,0:T(8,128)(2,1)}) %all-gather.11.cloned.1.call-update) | async-done | bytes 11534352 | tf_op jit(solution)/shard_map/all_gather | solution.py:95
  374.9 15.2 %copy.113 = bf16[2816,16,128]{0,2,1:T(8,128)(2,1)} copy(bf16[2816,16,128]{2,0,1:T(8,128)(2,1)} %bitcast.39) | data formatting | bytes 23068672 | tf_op jit(solution)/shard_map/reshape | solution.py:95
  390.1 126.8 %all-gather.7.cloned.1.call-done = bf16[2048,2816]{1,0:T(8,128)(2,1)} async-done(((bf16[128,2816]{1,0:T(8,128)(2,1)}), bf16[2048,2816]{1,0:T(8,128)(2,1)}) %all-gather.7.cloned.1.call-update) | async-done | bytes 11534352 | tf_op jit(solution)/shard_map/all_gather | solution.py:92
  516.9 9.7 %fusion.43 = f32[384,2816]{1,0:T(8,128)} fusion(bf16[2048,2816]{1,0:T(8,128)(2,1)} %all-gather.7.cloned.1.call-done, f32[384,2048]{1,0:T(8,128)S(1)} %get-tuple-element.61, f32[2048]{0:T(1024)S(1)} %copy-done.38, f32[384]{0:T(512)S(1)} %add_rsqrt_fusion), kind=kOutput, calls=%fused_computation.118 | convolution fusion | flops 4431544320 | bytes 19015168 | tf_op jit(solution)/shard_map/dot_general | solution.py:96
  526.6 132.3 %all-gather.9.cloned.1.call-done = bf16[2048,2816]{1,0:T(8,128)(2,1)} async-done(((bf16[128,2816]{1,0:T(8,128)(2,1)}), bf16[2048,2816]{1,0:T(8,128)(2,1)}) %all-gather.9.cloned.1.call-update) | async-done | bytes 11534352 | tf_op jit(solution)/shard_map/all_gather | solution.py:93
  658.9 21.5 %convolution_convert_fusion = bf16[384,2048]{1,0:T(8,128)(2,1)} fusion(bf16[2816,2048]{0,1:T(8,128)(2,1)} %bitcast.40, bf16[2048,2816]{1,0:T(8,128)(2,1)} %all-gather.9.cloned.1.call-done, f32[384,2816]{1,0:T(8,128)} %fusion.43, f32[384,2048]{1,0:T(8,128)S(1)} %get-tuple-element.61, f32[2048]{0:T(1024)S(1)} %copy-done.38, f32[384]{0:T(512)S(1)} %add_rsqrt_fusion), kind=kOutput, calls=%fused_computation.12 | convolution fusion | flops 8868003840 | bytes 32122368 | tf_op jit(solution)/shard_map/dot_general | solution.py:100
  680.4 7.4 %reduce-scatter.2.cloned.1.call-done = bf16[192,2048]{1,0:T(8,128)(2,1)} async-done(((bf16[384,2048]{1,0:T(8,128)(2,1)}), bf16[192,2048]{1,0:T(8,128)(2,1)}) %reduce-scatter.2.cloned.1.call-update) | async-done | bytes 786448 | tf_op jit(solution)/shard_map/reduce_scatter | solution.py:99
  689.2 2.4 fusion.8
  (206 shorter events, 58.0 us)
Async XLA Ops:
  7.4 10.4 %copy-start = (bf16[16,64,64]{2,1,0:T(8,128)(2,1)S(1)}, bf16[16,64,64]{2,1,0:T(8,128)(2,1)}, u32[]{:S(2)}) copy-start(bf16[16,64,64]{2,1,0:T(8,128)(2,1)} %param.21) | copy-start | bytes 393220
  7.4 243.6 %all-reduce.34.cloned.1.call-start = ((), (), s32[]{:S(2)}) async-start(), calls=%async_computation.1 | async-start | bytes 3145728 | tf_op jit(solution)/shard_map/psum | solution.py:85
  8.1 6.5 collective-permute-start
  19.6 1.7 copy-start.37
  29.9 4.5 copy-start.2
  116.5 5.7 copy-start.15
  116.5 5.7 copy-start.16
  116.5 5.7 copy-start.17
  116.5 6.0 copy-start.18
  116.5 6.0 copy-start.19
  116.5 6.0 copy-start.26
  116.5 6.0 copy-start.27
  118.8 3.8 copy-start.14
  118.8 3.9 copy-start.33
  118.8 3.9 copy-start.32
  121.6 2.1 copy-start.31
  122.2 1.6 copy-start.30
  122.6 1.3 copy-start.13
  122.8 1.2 copy-start.29
  123.7 0.7 copy-start.28
  124.0 0.9 copy-start.11
  124.0 1.0 copy-start.12
  124.5 0.7 copy-start.25
  125.0 0.7 copy-start.24
  125.7 1.0 copy-start.9
  125.7 1.2 copy-start.10
  126.9 0.7 copy-start.23
  128.0 3.1 copy-start.22
  132.5 1.4 copy-start.4
  132.5 1.6 copy-start.5
  134.1 1.4 copy-start.21
  135.6 3.2 copy-start.8
  135.6 46.1 %copy-start.7 = (f32[192,1024]{1,0:T(8,128)S(1)}, f32[192,1024]{1,0:T(8,128)}, u32[]{:S(2)}) copy-start(f32[192,1024]{1,0:T(8,128)} %add.291) | copy-start | bytes 2359300
  138.8 46.0 %copy-start.6 = (f32[191,1024]{1,0:T(8,128)S(1)}, f32[191,1024]{1,0:T(8,128)}, u32[]{:S(2)}) copy-start(f32[191,1024]{1,0:T(8,128)} %get-tuple-element.71) | copy-start | bytes 2347012
  138.8 46.0 %copy-start.20 = (f32[1,1024]{1,0:T(1,128)S(1)}, f32[1,1024]{1,0:T(1,128)}, u32[]{:S(2)}) copy-start(f32[1,1024]{1,0:T(1,128)} %slice.386) | copy-start | bytes 12292
  184.9 39.8 %copy-start.36 = (bf16[384,1024]{1,0:T(8,128)(2,1)S(1)}, bf16[384,1024]{1,0:T(8,128)(2,1)}, u32[]{:S(2)}) copy-start(bf16[384,1024]{1,0:T(8,128)(2,1)} %param.19) | copy-start | bytes 2359300
  231.8 143.1 %all-gather.11.cloned.1.call-start = ((), (), s32[]{:S(2)}) async-start(), calls=%async_computation.5 | async-start | bytes 12255232 | tf_op jit(solution)/shard_map/all_gather | solution.py:95
  232.3 20.5 %copy-start.34 = (f32[2048]{0:T(1024)S(1)}, f32[2048]{0:T(1024)}, u32[]{:S(2)}) copy-start(f32[2048]{0:T(1024)} %param.26) | copy-start | bytes 24580
  232.3 284.5 %all-gather.7.cloned.1.call-start = ((), (), s32[]{:S(2)}) async-start(), calls=%async_computation.2 | async-start | bytes 12255232 | tf_op jit(solution)/shard_map/all_gather | solution.py:92
  232.9 426.0 %all-gather.9.cloned.1.call-start = ((), (), s32[]{:S(2)}) async-start(), calls=%async_computation.3 | async-start | bytes 12255232 | tf_op jit(solution)/shard_map/all_gather | solution.py:93
  233.5 454.3 %reduce-scatter.2.cloned.1.call-start = ((), (), s32[]{:S(2)}) async-start(), calls=%async_computation.4 | async-start | bytes 2359296 | tf_op jit(solution)/shard_map/reduce_scatter | solution.py:99
  250.9 1.9 copy-start.3
  374.9 142.0 %copy-start.38 = (f32[2048]{0:T(1024)S(1)}, f32[2048]{0:T(1024)}, u32[]{:S(2)}) copy-start(f32[2048]{0:T(1024)} %param.27) | copy-start | bytes 24580
  680.4 8.8 %copy-start.35 = (f32[2048]{0:T(1024)S(1)}, f32[2048]{0:T(1024)}, u32[]{:S(2)}) copy-start(f32[2048]{0:T(1024)} %param.31) | copy-start | bytes 24580
  689.1 2.4 copy-start.1
Sparse Core Ops, SparseCore 0:
  231.9 19.0 all-reduce.33
  680.5 7.2 reduce-scatter.1
Sparse Core Ops, SparseCore 1:
  235.0 139.8 all-gather.10
  377.5 139.3 all-gather.6
  519.5 139.3 all-gather.8
